TPU v7x, 512 devices: a 4x2x32 block of a 4x8x32 slice. The times are simulated.
512 devices in a mesh: grp: 2 (over y), sp: 32 (over z), tp: 8 (over x, core).
Axes of the slice: x: 4, y: 2, z: 32, core: 2. Of those that a mesh axis runs over, the one named last changes fastest.
The devices are a block of a 4x8x32 slice.
Arguments:
- window_query: bfloat16 [20480, 2048], P(('grp', 'sp'), 'tp'), parts along dimension 0, may hold values from -24 to 24
- window_key: bfloat16 [20480, 1024], P(('grp', 'sp'), 'tp'), parts along dimension 0, may hold values from -24 to 24
- window_value: bfloat16 [20480, 1024], P(('grp', 'sp'), 'tp'), parts along dimension 0, may hold values from -6 to 6
- grid_query: bfloat16 [20480, 2048], P(('grp', 'sp'), 'tp'), parts along dimension 0, may hold values from -10 to 10
- grid_key: bfloat16 [20480, 1024], P(('grp', 'sp'), 'tp'), parts along dimension 0, may hold values from -10 to 10
- grid_value: bfloat16 [20480, 1024], P(('grp', 'sp'), 'tp'), parts along dimension 0, may hold values from -6 to 6
- sink_logit: float32 [16], P('tp'), may hold values from 1 to 6
- query_gain: float32 [128], replicated, may hold values from 0.8 to 6
- key_gain: float32 [128], replicated, may hold values from 0.8 to 6
- window_weights: bfloat16 [2048, 4096], P('tp'), may hold values from -0.59765625 to 0.59765625
- grid_weights: bfloat16 [2048, 4096], P('tp'), may hold values from -0.59765625 to 0.59765625
Outputs:
- merged: bfloat16 [20480, 4096], P(('grp', 'sp', 'tp')), parts along dimension 0
There are 2 independent parts, one for each index of `grp`. A program takes and returns all parts, laid end to end along the dimension named above; an argument that names none is the same for every part. Nothing has to cross between parts.
All inputs are finite; a program needn't handle non-finite values.
Results may differ from a plain program's by a relative error of at most 0.014.
The roundings to bfloat16 on the way count: a program that leaves them out, or rounds other values in their place, can miss the bound.
Values may be sent and summed in bfloat16 or wider, within the bound.
No kernel may reach another device: no remote copies, remote signals or barrier semaphores. Data moves between devices by JAX's collectives and lax.ppermute only.
A program may use at most 64 MiB of HBM per device.

v0:
```python
import jax
import jax.numpy as jnp
from jax import lax
from jax.sharding import PartitionSpec as P

HEAD = 128
QH_A = 16
WINDOW = 128
GRID_W = 64


THETA = 10000.0
NEGATIVE = -1e30
EPSILON = 1e-06


def extended(cells, sides, width):
    for axis, dim in sides:
        count = lax.axis_size(axis)
        ends = count - 1
        head = lax.slice_in_dim(cells, 0, width, axis=dim)
        tail = lax.slice_in_dim(cells, cells.shape[dim] - width, cells.shape[dim], axis=dim)
        cells = jnp.concatenate(
            [
                lax.ppermute(tail, axis, [(i, (i + 1) % count) for i in range(ends)]),
                cells,
                lax.ppermute(head, axis, [((i + 1) % count, i) for i in range(ends)]),
            ],
            axis=dim,
        )
    return cells


def sent_together(arrays, axis, dim, along):
    widths = [a.shape[along] for a in arrays]
    both = jnp.concatenate(arrays, axis=along)
    filled = lax.all_gather(both, axis, axis=dim, tiled=True)
    return tuple(jnp.split(filled, [sum(widths[:k]) for k in range(1, len(widths))], axis=along))


def in_blocks(value, dim, peers):
    dims = value.shape
    tiles = value.reshape(*dims[:dim], peers, dims[dim] // peers, *dims[dim + 1 :])
    return jnp.moveaxis(tiles, dim, 0)


def sent_and_summed(value, axis, dim):
    peers = lax.axis_size(axis)
    tiles = lax.all_to_all(in_blocks(value, dim, peers), axis, 0, 0, tiled=True)
    return jnp.sum(tiles.astype(jnp.float32), axis=0)


def turn_section(values, places):
    width = values.shape[-1]
    half_width = width // 2
    frequency = THETA ** (-jnp.arange(0, width, 2, dtype=jnp.float32) / width)
    angles = places[:, None] * frequency[None, :]
    cosine = jnp.cos(angles)[:, None, :]
    sine_part = jnp.sin(angles)[:, None, :]
    first_half = values[..., :half_width]
    second_half = values[..., half_width:]
    return jnp.concatenate(
        [
            first_half * cosine - second_half * sine_part,
            second_half * cosine + first_half * sine_part,
        ],
        axis=-1,
    )


def normed_turn(values, gain, places):
    count_rows = values.shape[0]
    shaped = values.astype(jnp.float32).reshape(count_rows, -1, HEAD)
    scaled = shaped * lax.rsqrt(jnp.mean(shaped * shaped, axis=-1, keepdims=True) + EPSILON)
    scaled = scaled * gain
    grid_row = (places // GRID_W).astype(jnp.float32)
    grid_col = (places % GRID_W).astype(jnp.float32)
    section = HEAD // 2
    turned = jnp.concatenate(
        [
            turn_section(scaled[..., :section], grid_row),
            turn_section(scaled[..., section:], grid_col),
        ],
        axis=-1,
    )
    return turned.astype(jnp.bfloat16)


def window_attend(queries, keys_pad, values_pad, slopes, sink_logits, offset, total_rows):
    query_rows = queries.shape[0]
    block_span = WINDOW // 2
    blocks = query_rows // block_span
    key_heads = keys_pad.shape[1] // HEAD
    group_size = queries.shape[1] // keys_pad.shape[1]
    query_blocks = queries.reshape(blocks, block_span, key_heads, group_size, HEAD)
    key_blocks = keys_pad.reshape(blocks + 4, block_span, key_heads, HEAD)
    value_blocks = values_pad.reshape(blocks + 4, block_span, key_heads, HEAD)
    key_window = jnp.concatenate(
        [key_blocks[block_shift : block_shift + blocks] for block_shift in range(5)], axis=1
    )
    value_window = jnp.concatenate(
        [value_blocks[block_shift : block_shift + blocks] for block_shift in range(5)], axis=1
    )
    scores = jnp.einsum(
        "nqkgd,nskd->kgnqs", query_blocks, key_window, preferred_element_type=jnp.float32
    ) * HEAD ** (-0.5)
    query_place = offset + jnp.arange(query_rows, dtype=jnp.int32).reshape(blocks, block_span, 1)
    key_place = (
        offset
        - WINDOW
        + block_span * jnp.arange(blocks, dtype=jnp.int32)[:, None, None]
        + jnp.arange(5 * block_span, dtype=jnp.int32)[None, None, :]
    )
    distance = jnp.abs(key_place - query_place)
    inside = (distance <= WINDOW) & (key_place >= 0) & (key_place < total_rows)
    slope_grid = slopes.reshape(key_heads, group_size, 1, 1, 1)
    sink_grid = sink_logits.reshape(key_heads, group_size, 1, 1)
    scores = jnp.where(inside, scores - slope_grid * distance.astype(jnp.float32), NEGATIVE)
    highest = jnp.maximum(jnp.max(scores, axis=-1), sink_grid)
    raised = jnp.exp(scores - highest[..., None])
    denominator = jnp.sum(raised, axis=-1) + jnp.exp(sink_grid - highest)
    weights = (raised / denominator[..., None]).astype(jnp.bfloat16)
    attended = jnp.einsum(
        "kgnqs,nskd->nqkgd", weights, value_window, preferred_element_type=jnp.float32
    )
    return attended.astype(jnp.bfloat16).reshape(query_rows, -1)


def absorb_keys(carry, queries, key_block, value_block):
    highest, summed, gathered = carry
    scores = jnp.einsum(
        "tkgd,skd->kgts", queries, key_block, preferred_element_type=jnp.float32
    ) * HEAD ** (-0.5)
    raised_top = jnp.maximum(highest, jnp.max(scores, axis=-1))
    fading = jnp.exp(highest - raised_top)
    raised = jnp.exp(scores - raised_top[..., None])
    summed = summed * fading + jnp.sum(raised, axis=-1)
    gathered = gathered * fading[..., None] + jnp.einsum(
        "kgts,skd->kgtd",
        raised.astype(jnp.bfloat16),
        value_block,
        preferred_element_type=jnp.float32,
    )
    return (raised_top, summed, gathered)


def sweep_keys(carry, queries, key_rows, value_rows):
    count_rows = key_rows.shape[0]
    block_rows = count_rows
    while block_rows > 1024 and block_rows % 2 == 0:
        block_rows = block_rows // 2
    key_heads = queries.shape[1]
    key_blocks = key_rows.reshape(count_rows // block_rows, block_rows, key_heads, HEAD)
    value_blocks = value_rows.reshape(count_rows // block_rows, block_rows, key_heads, HEAD)

    def scan_step(inner, block_pair):
        return (absorb_keys(inner, queries, block_pair[0], block_pair[1]), None)

    result, _ = lax.scan(scan_step, carry, (key_blocks, value_blocks))
    return result


def per_device(
    window_query,
    window_key,
    window_value,
    grid_query,
    grid_key,
    grid_value,
    sink_logit,
    query_gain,
    key_gain,
    window_weights,
    grid_weights,
):
    local_rows = window_query.shape[0]
    offset = lax.axis_index("sp") * local_rows
    total_rows = local_rows * lax.axis_size("sp")
    local_heads = sink_logit.shape[0]
    head_number = lax.axis_index("tp") * local_heads + 1 + jnp.arange(local_heads, dtype=jnp.int32)
    slopes = 2.0 ** (-8.0 * head_number.astype(jnp.float32) / QH_A)
    stacked = jnp.stack([window_key, window_value])
    padded = extended(stacked, (("sp", 1),), WINDOW)
    window_out = window_attend(
        window_query, padded[0], padded[1], slopes, sink_logit, offset, total_rows
    )
    places = offset + jnp.arange(local_rows, dtype=jnp.int32)
    key_heads = grid_key.shape[1] // HEAD
    group_size = grid_query.shape[1] // grid_key.shape[1]
    turned_q = normed_turn(grid_query, query_gain, places).reshape(
        local_rows, key_heads, group_size, HEAD
    )
    turned_k = normed_turn(grid_key, key_gain, places).reshape(local_rows, key_heads * HEAD)
    start_carry = (
        jnp.full((key_heads, group_size, local_rows), NEGATIVE, jnp.float32),
        jnp.zeros((key_heads, group_size, local_rows), jnp.float32),
        jnp.zeros((key_heads, group_size, local_rows, HEAD), jnp.float32),
    )
    block_pair = sent_together((turned_k, grid_value), "sp", 0, 1)
    final_carry = sweep_keys(start_carry, turned_q, block_pair[0], block_pair[1])
    grid_out = (final_carry[2] / final_carry[1][..., None]).astype(jnp.bfloat16)
    shaped_b = grid_weights.reshape(key_heads, group_size, HEAD, grid_weights.shape[1])
    projected = jnp.dot(window_out, window_weights, preferred_element_type=jnp.float32)
    merged = sent_and_summed(
        (
            projected
            + jnp.einsum("kgtd,kgdo->to", grid_out, shaped_b, preferred_element_type=jnp.float32)
        ).astype(jnp.bfloat16),
        "tp",
        0,
    )
    return merged.astype(jnp.bfloat16)


def solution(mesh):
    return jax.shard_map(
        per_device,
        mesh=mesh,
        in_specs=(
            P(("grp", "sp"), "tp"),
            P(("grp", "sp"), "tp"),
            P(("grp", "sp"), "tp"),
            P(("grp", "sp"), "tp"),
            P(("grp", "sp"), "tp"),
            P(("grp", "sp"), "tp"),
            P("tp"),
            P(),
            P(),
            P("tp", None),
            P("tp", None),
        ),
        out_specs=P(("grp", "sp", "tp"), None),
        check_vma=False,
    )
```

profile of v0, /device:TPU:33, one launch (start us, length us, event | category | flops | bytes accessed | tf_op | source)
XLA Modules:
  0.0 315.7 jit_solution(17396354248166737223)
XLA Ops:
  12.8 5.2 %collective-permute-start = (bf16[2,128,128]{2,1,0:T(8,128)(2,1)}, bf16[2,128,128]{2,1,0:T(8,128)(2,1)S(1)}, u32[]{:S(2)}, u32[]{:S(2)}) collective-permute-start(bf16[2,128,128]{2,1,0:T(8,128)(2,1)} %get-tuple-element.133), channel_id=1, source_target_pairs={{0,8},{8,16},{16,24},{24,32},{32,40},{40,48},{48,56},{56,64},{64,7... | collective-permute-start | bytes 196616 | tf_op jit(solution)/shard_map/ppermute | solution.py:25
  27.7 133.3 %all-gather.2.cloned.1.call-done = bf16[10240,256]{1,0:T(8,128)(2,1)} async-done(((bf16[320,256]{1,0:T(8,128)(2,1)}), bf16[10240,256]{1,0:T(8,128)(2,1)}) %all-gather.2.cloned.1.call-update) | async-done | bytes 5242896 | tf_op jit(solution)/shard_map/all_gather | solution.py:37
  161.1 4.2 %fusion.69 = (bf16[10240,128]{1,0:T(8,128)(2,1)}, bf16[10240,128]{1,0:T(8,128)(2,1)}) fusion(bf16[10240,256]{1,0:T(8,128)(2,1)} %all-gather.2.cloned.1.call-done), kind=kLoop, calls=%fused_computation.132 | loop fusion | bytes 10485760 | tf_op jit(solution)/shard_map/split | solution.py:38
  165.3 81.1 %while.15 = (s32[]{:T(128)}, f32[1,2,320]{2,1,0:T(2,128)S(1)}, f32[1,2,320]{2,1,0:T(2,128)S(1)}, f32[1,2,320,128]{3,2,1,0:T(8,128)S(1)}, bf16[16,640,1,128]{3,1,...) while((s32[]{:T(128)}, f32[1,2,320]{2,1,0:T(2,128)S(1)}, ...), condition=%wide.region_7.8_spmd.clone, body=%wide.region_4.7_spmd.clone.sunk | while | flops 213241600 | bytes 12657797 | solution.py:159
  165.3 2.5 bitcast_reduce_fusion.2
  167.7 2.1 fusion.84
  170.3 2.5 bitcast_reduce_fusion.2
  172.8 2.1 fusion.84
  175.4 2.5 bitcast_reduce_fusion.2
  177.9 2.1 fusion.84
  180.5 2.5 bitcast_reduce_fusion.2
  182.9 2.1 fusion.84
  185.5 2.5 bitcast_reduce_fusion.2
  188.0 2.1 fusion.84
  190.6 2.5 bitcast_reduce_fusion.2
  193.1 2.1 fusion.84
  195.7 2.5 bitcast_reduce_fusion.2
  198.2 2.1 fusion.84
  200.7 2.5 bitcast_reduce_fusion.2
  203.2 2.1 fusion.84
  205.8 2.5 bitcast_reduce_fusion.2
  208.3 2.1 fusion.84
  210.9 2.5 bitcast_reduce_fusion.2
  215.9 2.5 bitcast_reduce_fusion.2
  218.4 2.1 fusion.84
  221.0 2.5 bitcast_reduce_fusion.2
  226.1 2.5 bitcast_reduce_fusion.2
  231.2 2.5 bitcast_reduce_fusion.2
  236.2 2.5 bitcast_reduce_fusion.2
  241.3 2.5 bitcast_reduce_fusion.2
  248.8 57.1 %all_to_all.5 = bf16[8,40,4096]{2,1,0:T(8,128)(2,1)} all-to-all(bf16[8,40,4096]{2,1,0:T(8,128)(2,1)S(1)} %bitcast.146), channel_id=1, replica_groups=mesh['grp'=2,'sp'=32,'tp'=8] {'tp'}, dimensions={0} | all-to-all | bytes 5242880 | tf_op jit(solution)/shard_map/all_to_all | solution.py:49
  305.9 2.9 reduce_sum.53
  (170 shorter events, 38.3 us)
Async XLA Ops:
  6.5 239.8 %copy-start = (bf16[256,4096]{1,0:T(8,128)(2,1)S(1)}, bf16[256,4096]{1,0:T(8,128)(2,1)}, u32[]{:S(2)}) copy-start(bf16[256,4096]{1,0:T(8,128)(2,1)} %param.23) | copy-start | bytes 6291460
  6.6 5.6 %copy-start.3 = (bf16[320,128]{1,0:T(8,128)(2,1)S(1)}, bf16[320,128]{1,0:T(8,128)(2,1)}, u32[]{:S(2)}) copy-start(bf16[320,128]{1,0:T(8,128)(2,1)} %param.14) | copy-start | bytes 245764
  6.6 5.6 %copy-start.4 = (bf16[320,128]{1,0:T(8,128)(2,1)S(1)}, bf16[320,128]{1,0:T(8,128)(2,1)}, u32[]{:S(2)}) copy-start(bf16[320,128]{1,0:T(8,128)(2,1)} %param.15) | copy-start | bytes 245764
  6.6 12.9 %copy-start.5 = (bf16[320,256]{1,0:T(8,128)(2,1)S(1)}, bf16[320,256]{1,0:T(8,128)(2,1)}, u32[]{:S(2)}) copy-start(bf16[320,256]{1,0:T(8,128)(2,1)} %param.13) | copy-start | bytes 491524
  6.6 12.9 %copy-start.6 = (bf16[320,256]{1,0:T(8,128)(2,1)S(1)}, bf16[320,256]{1,0:T(8,128)(2,1)}, u32[]{:S(2)}) copy-start(bf16[320,256]{1,0:T(8,128)(2,1)} %param.16) | copy-start | bytes 491524
  6.6 154.5 %all-gather.2.cloned.1.call-start = ((), (), s32[]{:S(2)}) async-start(), calls=%async_computation.1 | async-start | bytes 5406720 | tf_op jit(solution)/shard_map/all_gather | solution.py:37
  6.6 6.2 %copy-start.7 = (f32[32]{0:T(128)}, f32[32]{0:T(128)S(1)}, u32[]{:S(2)}) copy-start(f32[32]{0:T(128)S(1)} %multiply_power_fusion) | copy-start | bytes 388
  12.8 12.9 %collective-permute-start = (bf16[2,128,128]{2,1,0:T(8,128)(2,1)}, bf16[2,128,128]{2,1,0:T(8,128)(2,1)S(1)}, u32[]{:S(2)}, u32[]{:S(2)}) collective-permute-start(bf16[2,128,128]{2,1,0:T(8,128)(2,1)} %get-tuple-element.133), channel_id=1, source_target_pairs={{0,8},{8,16},{16,24},{24,32},{32,40},{40,48},{48,56},{56,64},{64,7... | collective-permute-start | bytes 196616 | tf_op jit(solution)/shard_map/ppermute | solution.py:25
  18.1 7.7 %collective-permute-start.1 = (bf16[2,128,128]{2,1,0:T(8,128)(2,1)}, bf16[2,128,128]{2,1,0:T(8,128)(2,1)S(1)}, u32[]{:S(2)}, u32[]{:S(2)}) collective-permute-start(bf16[2,128,128]{2,1,0:T(8,128)(2,1)} %get-tuple-element.132), channel_id=1, source_target_pairs={{8,0},{16,8},{24,16},{32,24},{40,32},{48,40},{56,48},{64,56},{72,6... | collective-permute-start | bytes 196616 | tf_op jit(solution)/shard_map/ppermute | solution.py:27
  25.9 0.7 copy-start.8
  167.7 2.1 copy-start.1
  172.8 2.1 copy-start.1
  177.9 2.1 copy-start.1
  182.9 2.1 copy-start.1
  188.0 2.1 copy-start.1
  193.1 2.1 copy-start.1
  198.1 2.1 copy-start.1
  203.2 2.1 copy-start.1
  208.3 2.1 copy-start.1
  213.3 2.1 copy-start.1
  218.4 2.1 copy-start.1
  223.5 2.1 copy-start.1
  228.6 2.1 copy-start.1
  233.6 2.1 copy-start.1
  238.7 2.1 copy-start.1
  243.8 2.1 copy-start.1
  246.4 1.6 copy-start.2
Sparse Core Ops, SparseCore 0:
  12.3 148.7 all-gather.1
where the time goes:
time: 316 us
  waiting for transfers between devices  133 us (42%)
  matrix products  75.3 us (24%)
  blocking collectives  57.1 us (18%)
  other arithmetic  21.5 us (7%)
  between operations  13.8 us (4%)
  local copies, waits for them, and re-layouts  7.34 us (2%)
  starting transfers between devices  6.61 us (2%)
    all_gather x1, waiting for transfers between devices, sent_together(): filled = lax.all_gather(both, axis, axis=dim, tiled=True)  133 us
    all_to_all x1, blocking collectives, sent_and_summed(): tiles = lax.all_to_all(in_blocks(value, dim, peers), axis, 0, 0, tiled=True)  57.1 us
    dot_general x16, matrix products, absorb_keys(): jnp.einsum('tkgd,skd->kgts', queries, key_block, preferred_element_type=j...  39.4 us
    dot_general x16, matrix products, absorb_keys(): jnp.einsum('kgts,skd->kgtd', raised.astype(jnp.bfloat16), value_block, pr...  33.2 us
    reduce_sum x16, other arithmetic, absorb_keys(): summed = summed * fading + jnp.sum(raised, axis=-1)  7.23 us
  transfers between devices with their start and end apart: 3, of which 1 were waited for; matrix products, arithmetic and copies ran while one was open for 3% of the time, Pallas kernels for 0%

commit v1 on v0

v1 whole, which is shorter than its diff:
```python
import functools
import math

import jax
import jax.numpy as jnp
from jax import lax
from jax.experimental import pallas as pl
from jax.experimental.pallas import tpu as pltpu
from jax.sharding import Mesh
from jax.sharding import PartitionSpec as P

HEAD = 128
QH_A = 16
WINDOW = 128
GRID_W = 64
THETA = 10000.0
NEGATIVE = -1e30
EPSILON = 1e-06
CORES = 2
PLANES = 2


def turn_tables(offset, local_rows):
    half = HEAD // 4
    frequency = THETA ** (-jnp.arange(0, HEAD // 2, 2, dtype=jnp.float32) / (HEAD // 2))
    places = offset + jnp.arange(local_rows, dtype=jnp.int32)
    row = (places // GRID_W).astype(jnp.float32)[:, None] * frequency[None, :]
    col = (places % GRID_W).astype(jnp.float32)[:, None] * frequency[None, :]
    angles = jnp.concatenate([row, row, col, col], axis=-1)
    lane = jnp.arange(HEAD, dtype=jnp.int32) % (2 * half)
    sign = jnp.where(lane < half, -1.0, 1.0).astype(jnp.float32)
    return jnp.cos(angles), jnp.sin(angles) * sign


def turn_kernel(x_ref, gain_ref, cos_ref, sin_ref, *rest):
    o_ref = rest[-1]
    width = x_ref.shape[1]
    lane = lax.broadcasted_iota(jnp.int32, (x_ref.shape[0], HEAD), 1) % (HEAD // 2)
    for k in range(width // HEAD):
        x = x_ref[:, k * HEAD : (k + 1) * HEAD].astype(jnp.float32)
        scaled = x * lax.rsqrt(jnp.mean(x * x, axis=-1, keepdims=True) + EPSILON)
        scaled = scaled * gain_ref[...]
        up = pltpu.roll(scaled, HEAD // 4, axis=1)
        down = pltpu.roll(scaled, HEAD - HEAD // 4, axis=1)
        other = jnp.where(lane < HEAD // 4, down, up)
        turned = scaled * cos_ref[...] + other * sin_ref[...]
        o_ref[:, k * HEAD : (k + 1) * HEAD] = turned.astype(jnp.bfloat16)
    if len(rest) == 2:
        o_ref[:, width:] = rest[0][...]


def turn(x, gain, cos, sin, beside=None):
    rows, width = x.shape
    args = [x, gain.reshape(1, HEAD), cos, sin]
    if beside is not None:
        args.append(beside)
        width = width + beside.shape[1]
    return pl.pallas_call(
        turn_kernel,
        out_shape=jax.ShapeDtypeStruct((rows, width), jnp.bfloat16),
        cost_estimate=pl.CostEstimate(
            flops=rows * width * 16, bytes_accessed=rows * width * 8, transcendentals=rows
        ),
    )(*args)


def attend_kernel(q_ref, kv_ref, o_ref, rows_ref, top_ref, sum_ref, acc_ref, *, chunks):
    step = pl.program_id(0)
    heads = q_ref.shape[1] // HEAD
    count = q_ref.shape[0]
    factor = math.log2(math.e) * HEAD ** (-0.5)

    @pl.when(step == 0)
    def _():
        for h in range(heads):
            rows_ref[h * count : (h + 1) * count, :] = q_ref[:, h * HEAD : (h + 1) * HEAD]
        top_ref[...] = jnp.full_like(top_ref, NEGATIVE)
        sum_ref[...] = jnp.zeros_like(sum_ref)
        acc_ref[...] = jnp.zeros_like(acc_ref)

    keys = kv_ref[:, :HEAD]
    values = kv_ref[:, HEAD:].T

    def score(lo, hi):
        return lax.dot_general(
            keys,
            rows_ref[lo:hi, :],
            (((1,), (1,)), ((), ())),
            preferred_element_type=jnp.float32,
        )

    def absorb(scores, lo, hi):
        before = top_ref[:, lo:hi]
        top = jnp.maximum(before, jnp.max(scores, axis=0, keepdims=True))
        fading = jnp.exp2((before - top) * factor)
        raised = jnp.exp2((scores - top) * factor)
        top_ref[:, lo:hi] = top
        sum_ref[:, lo:hi] = sum_ref[:, lo:hi] * fading + jnp.sum(raised, axis=0, keepdims=True)
        acc_ref[:, lo:hi] = acc_ref[:, lo:hi] * fading + lax.dot_general(
            values,
            raised.astype(jnp.bfloat16),
            (((1,), (0,)), ((), ())),
            preferred_element_type=jnp.float32,
        )

    waiting = None
    for lo, hi in chunks:
        scores = score(lo, hi)
        if waiting is not None:
            absorb(*waiting)
        waiting = (scores, lo, hi)
    absorb(*waiting)

    @pl.when(step == pl.num_programs(0) - 1)
    def _():
        out = (acc_ref[...] / sum_ref[...]).T.astype(jnp.bfloat16)
        for h in range(heads):
            o_ref[:, h * HEAD : (h + 1) * HEAD] = out[h * count : (h + 1) * count, :]


def attend(queries, kv, block=1024, chunk=256):
    count, width = queries.shape
    total = kv.shape[0]
    while total % block:
        block //= 2
    rows = count * (width // HEAD)
    chunks = tuple((lo, min(lo + chunk, rows)) for lo in range(0, rows, chunk))
    return pl.pallas_call(
        functools.partial(attend_kernel, chunks=chunks),
        grid=(total // block,),
        in_specs=[
            pl.BlockSpec((count, width), lambda i: (0, 0)),
            pl.BlockSpec((block, 2 * HEAD), lambda i: (i, 0)),
        ],
        out_specs=pl.BlockSpec((count, width), lambda i: (0, 0)),
        out_shape=jax.ShapeDtypeStruct((count, width), jnp.bfloat16),
        scratch_shapes=[
            pltpu.VMEM((rows, HEAD), jnp.bfloat16),
            pltpu.VMEM((1, rows), jnp.float32),
            pltpu.VMEM((1, rows), jnp.float32),
            pltpu.VMEM((HEAD, rows), jnp.float32),
        ],
        compiler_params=pltpu.CompilerParams(dimension_semantics=("arbitrary",)),
        cost_estimate=pl.CostEstimate(
            flops=4 * rows * total * HEAD,
            bytes_accessed=total * 2 * HEAD * 2,
            transcendentals=rows * total,
        ),
    )(queries, kv)


def extended(cells, axes, width):
    count = math.prod(lax.axis_size(a) for a in axes)
    ends = count - 1
    head = cells[:, :width]
    tail = cells[:, cells.shape[1] - width :]
    return jnp.concatenate(
        [
            lax.ppermute(tail, axes, [(i, i + 1) for i in range(ends)]),
            cells,
            lax.ppermute(head, axes, [(i + 1, i) for i in range(ends)]),
        ],
        axis=1,
    )


def window_attend(queries, keys_pad, values_pad, slopes, sink_logits, offset, total_rows):
    query_rows = queries.shape[0]
    block_span = WINDOW // 2
    blocks = query_rows // block_span
    key_heads = keys_pad.shape[1] // HEAD
    group_size = queries.shape[1] // keys_pad.shape[1]
    query_blocks = queries.reshape(blocks, block_span, key_heads, group_size, HEAD)
    key_blocks = keys_pad.reshape(blocks + 4, block_span, key_heads, HEAD)
    value_blocks = values_pad.reshape(blocks + 4, block_span, key_heads, HEAD)
    key_window = jnp.concatenate([key_blocks[s : s + blocks] for s in range(5)], axis=1)
    value_window = jnp.concatenate([value_blocks[s : s + blocks] for s in range(5)], axis=1)
    scores = jnp.einsum(
        "nqkgd,nskd->kgnqs", query_blocks, key_window, preferred_element_type=jnp.float32
    ) * HEAD ** (-0.5)
    query_place = offset + jnp.arange(query_rows, dtype=jnp.int32).reshape(blocks, block_span, 1)
    key_place = (
        offset
        - WINDOW
        + block_span * jnp.arange(blocks, dtype=jnp.int32)[:, None, None]
        + jnp.arange(5 * block_span, dtype=jnp.int32)[None, None, :]
    )
    distance = jnp.abs(key_place - query_place)
    inside = (distance <= WINDOW) & (key_place >= 0) & (key_place < total_rows)
    slope_grid = slopes.reshape(key_heads, group_size, 1, 1, 1)
    sink_grid = sink_logits.reshape(key_heads, group_size, 1, 1)
    scores = jnp.where(inside, scores - slope_grid * distance.astype(jnp.float32), NEGATIVE)
    highest = jnp.maximum(jnp.max(scores, axis=-1), sink_grid)
    raised = jnp.exp(scores - highest[..., None])
    denominator = jnp.sum(raised, axis=-1) + jnp.exp(sink_grid - highest)
    weights = (raised / denominator[..., None]).astype(jnp.bfloat16)
    attended = jnp.einsum(
        "kgnqs,nskd->nqkgd", weights, value_window, preferred_element_type=jnp.float32
    )
    return attended.astype(jnp.bfloat16).reshape(query_rows, -1)


def by_target(rows):
    across = lax.axis_size("x")
    x = lax.axis_index("x")
    core = lax.axis_index("core")
    count = rows.shape[0] // (across * CORES)
    tiles = rows.reshape(across, CORES, count, rows.shape[1])
    tiles = jnp.where(core == 0, tiles, tiles[:, ::-1])
    tiles = lax.dynamic_slice_in_dim(jnp.concatenate([tiles, tiles], axis=0), x, across, axis=0)
    return jnp.swapaxes(tiles, 0, 1).reshape(rows.shape)


def swapped(value):
    across = lax.axis_size("x")
    index = lambda plane, x, core: (plane * across + x) * CORES + core
    pairs = [
        (index(p, x, c), index(c, x, p))
        for p in range(PLANES)
        for x in range(across)
        for c in range(CORES)
    ]
    return lax.ppermute(value, ("lo", "x", "core"), pairs)


def sent_and_summed(partial):
    half = partial.shape[0] // CORES
    across = lax.axis_size("x")
    theirs = lax.ppermute(partial[half:], "core", [(0, 1), (1, 0)])
    both = partial[:half].astype(jnp.float32) + theirs.astype(jnp.float32)
    tiles = both.astype(jnp.bfloat16).reshape(across, half // across, -1)
    total = tiles[0].astype(jnp.float32)
    for d in range(1, across):
        total = total + lax.ppermute(
            tiles[d], "x", [(i, (i + d) % across) for i in range(across)]
        ).astype(jnp.float32)
    return total


def per_device(
    window_query,
    window_key,
    window_value,
    grid_query,
    grid_key,
    grid_value,
    sink_logit,
    query_gain,
    key_gain,
    window_weights,
    grid_weights,
):
    local_rows = window_query.shape[0]
    planes = ("hi", "lo")
    plane = lax.axis_index("hi") * PLANES + lax.axis_index("lo")
    head_group = lax.axis_index("x") * CORES + lax.axis_index("core")
    offset = plane * local_rows
    total_rows = local_rows * lax.axis_size("hi") * PLANES
    cos, sin = turn_tables(offset, local_rows)
    kv = swapped(turn(grid_key, key_gain, cos, sin, grid_value))
    kv_all = lax.all_gather(kv, ("hi", "core"), axis=0, tiled=True)

    kv, cos, sin, grid_query, window_query = lax.optimization_barrier(
        (kv, cos, sin, grid_query, window_query)
    )
    queries = swapped(by_target(turn(grid_query, query_gain, cos, sin)))

    local_heads = sink_logit.shape[0]
    head_number = head_group * local_heads + 1 + jnp.arange(local_heads, dtype=jnp.int32)
    slopes = 2.0 ** (-8.0 * head_number.astype(jnp.float32) / QH_A)
    padded = extended(jnp.stack([window_key, window_value]), planes, WINDOW)
    window_out = by_target(
        window_attend(window_query, padded[0], padded[1], slopes, sink_logit, offset, total_rows)
    )
    grid_out = swapped(attend(queries, kv_all))
    partial = jnp.dot(window_out, window_weights, preferred_element_type=jnp.float32) + jnp.dot(
        grid_out, grid_weights, preferred_element_type=jnp.float32
    )
    return sent_and_summed(partial.astype(jnp.bfloat16)).astype(jnp.bfloat16)


def solution(mesh):
    shape = mesh.shape
    inner = Mesh(
        mesh.devices.reshape(
            shape["grp"], shape["sp"] // PLANES, PLANES, shape["tp"] // CORES, CORES
        ),
        ("grp", "hi", "lo", "x", "core"),
    )
    rows = ("grp", "hi", "lo")
    heads = ("x", "core")
    return jax.shard_map(
        per_device,
        mesh=inner,
        in_specs=(
            P(rows, heads),
            P(rows, heads),
            P(rows, heads),
            P(rows, heads),
            P(rows, heads),
            P(rows, heads),
            P(heads),
            P(),
            P(),
            P(heads, None),
            P(heads, None),
        ),
        out_specs=P(rows + heads, None),
        check_vma=False,
    )
```

time: 316 us -> 212 us (0.67)
  matrix products: 75.3 us -> 2.56 us
  blocking collectives: 57.1 us -> 0 us
  starting transfers between devices: 6.61 us -> 63 us
  waiting for transfers between devices: 133 us -> 105 us
  Pallas kernels: 0 us -> 17.7 us
  other arithmetic: 21.5 us -> 6.11 us
  local copies, waits for them, and re-layouts: 7.34 us -> 2.13 us
    dot_general x33 -> x1, matrix products: 73.6 us -> 0.86 us  [per_device(): jnp.dot(grid_out, grid_weights, preferred_element_type=jnp.float32)]
    all_to_all x1 -> x0, blocking collectives: 57.1 us -> none  [sent_and_summed(): tiles = lax.all_to_all(in_blocks(value, dim, peers), axis, 0, 0, tiled=True)]
    ppermute x2 -> x9, starting transfers between devices: 6.55 us -> 63 us  [the longest x3 46.8 us: swapped(): return lax.ppermute(value, ('lo', 'x', 'core'), pairs)]
    all_gather x1, waiting for transfers between devices: 133 us -> 80.4 us  [per_device(): kv_all = lax.all_gather(kv, ('hi', 'core'), axis=0, tiled=True)]
    ppermute x2 -> x9, waiting for transfers between devices: 0.01 us -> 25.1 us  [the longest x3 11.2 us: sent_and_summed(): lax.ppermute(tiles[d], 'x', [(i, (i + d) % across) for i in range(across)])]
    pallas_call x0 -> x3, Pallas kernels: none -> 17.7 us  [the longest x1 13.5 us: attend(): pl.pallas_call(functools.partial(attend_kernel, chunks=chunks), grid=(tot...]
    reduce_sum x19 -> x0, other arithmetic: 11.8 us -> none  [the longest x16 7.23 us: absorb_keys(): summed = summed * fading + jnp.sum(raised, axis=-1)]
    split x1 -> x0, local copies, waits for them, and re-layouts: 4.16 us -> none  [sent_together(): jnp.split(filled, [sum(widths[:k]) for k in range(1, len(widths))], axis=...]
  transfers between devices with their start and end apart: 3 -> 10, of which waited for: 1 -> 8; matrix products, arithmetic and copies ran while one was open for 3% -> 3% of each run, Pallas kernels for 0% -> 1%
where the time goes in v1:
time: 212 us; the launch traced here: 211 us
  waiting for transfers between devices  105 us (50%)
  starting transfers between devices  63 us (30%)
  Pallas kernels  17.7 us (8%)
  between operations  13.8 us (7%)
  other arithmetic  6.11 us (3%)
  matrix products  2.56 us (1%)
  local copies, waits for them, and re-layouts  2.13 us (1%)
    all_gather x1, waiting for transfers between devices, per_device(): kv_all = lax.all_gather(kv, ('hi', 'core'), axis=0, tiled=True)  80.4 us
    ppermute x3, starting transfers between devices, swapped(): return lax.ppermute(value, ('lo', 'x', 'core'), pairs)  46.8 us
    pallas_call x1, Pallas kernels, attend(): pl.pallas_call(functools.partial(attend_kernel, chunks=chunks), grid=(tot...  13.5 us
    ppermute x3, waiting for transfers between devices, sent_and_summed(): lax.ppermute(tiles[d], 'x', [(i, (i + d) % across) for i in range(across)])  11.2 us
    ppermute x3, waiting for transfers between devices, swapped(): return lax.ppermute(value, ('lo', 'x', 'core'), pairs)  10.2 us
    ppermute x3, starting transfers between devices, sent_and_summed(): lax.ppermute(tiles[d], 'x', [(i, (i + d) % across) for i in range(across)])  8.9 us
  transfers between devices with their start and end apart: 10, of which 8 were waited for; matrix products, arithmetic and copies ran while one was open for 3% of the time, Pallas kernels for 1%

profile of v1, /device:TPU:33, one launch (start us, length us, event | category | flops | bytes accessed | tf_op | source)
XLA Modules:
  0.0 210.8 jit_solution(11289158876658629912)
XLA Ops:
  6.8 1.4 sine_multiply_fusion
  8.2 2.0 shard_map.109
  10.2 5.7 %collective-permute-start.2 = (bf16[320,256]{1,0:T(8,128)(2,1)}, bf16[320,256]{1,0:T(8,128)(2,1)S(1)}, u32[]{:S(2)}, u32[]{:S(2)}) collective-permute-start(bf16[320,256]{1,0:T(8,128)(2,1)} %shard_map.109), channel_id=1, source_target_pairs={{0,0},{1,8},{2,2},{3,10},{4,4},{5,12},{6,6},{7,14},{8,1},{9,9},{10... | collective-permute-start | bytes 491528 | tf_op jit(solution)/shard_map/ppermute | solution.py:223
  15.9 3.2 %collective-permute-done.2 = bf16[320,256]{1,0:T(8,128)(2,1)S(1)} collective-permute-done((bf16[320,256]{1,0:T(8,128)(2,1)}, bf16[320,256]{1,0:T(8,128)(2,1)S(1)}, u32[]{:S(2)}, u32[]{:S(2)}) %collective-permute-start.2) | collective-permute-done | bytes 163872 | tf_op jit(solution)/shard_map/ppermute | solution.py:223
  19.1 0.7 copy-done.5
  19.9 0.8 pad_maximum_fusion.2
  20.7 1.3 collective-permute-start.1
  22.0 4.0 %collective-permute-start = (bf16[2,128,128]{2,1,0:T(8,128)(2,1)S(1)}, bf16[2,128,128]{2,1,0:T(8,128)(2,1)S(1)}, u32[]{:S(2)}, u32[]{:S(2)}) collective-permute-start(bf16[2,128,128]{2,1,0:T(8,128)(2,1)S(1)} %get-tuple-element.29), channel_id=1, source_target_pairs={{0,8},{8,16},{16,24},{24,32},{32,40},{40,48},{48,56},{56,64},{64,7... | collective-permute-start | bytes 196616 | tf_op jit(solution)/shard_map/ppermute | solution.py:159
  26.7 0.7 collective-permute-done
  27.7 0.7 copy-done.6
  28.5 2.2 %shard_map.110 = bf16[320,256]{1,0:T(8,128)(2,1)} custom-call(bf16[320,256]{1,0:T(8,128)(2,1)} %x_ref.2, f32[1,128]{1,0:T(1,128)} %bitcast.74, f32[320,128]{1,0:T(8,128)} %get-tuple-element.11.cos_ref, f32[320,128]{1,0:T(8,128)} %get-tuple-element.12.sin_ref), custom_call_target="tpu_custom_call" | custom-call | flops 1310720 | bytes 655360 | tf_op jit(solution)/shard_map/pallas_call | solution.py:58
  30.7 1.1 reverse_select_fusion
  31.9 39.1 %collective-permute-start.3 = (bf16[320,256]{1,0:T(8,128)(2,1)S(1)}, bf16[320,256]{1,0:T(8,128)(2,1)}, u32[]{:S(2)}, u32[]{:S(2)}) collective-permute-start(bf16[320,256]{1,0:T(8,128)(2,1)S(1)} %bitcast.72), channel_id=1, source_target_pairs={{0,0},{1,8},{2,2},{3,10},{4,4},{5,12},{6,6},{7,14},{8,1},{9,9},{10... | collective-permute-start | bytes 491528 | tf_op jit(solution)/shard_map/ppermute | solution.py:223
  71.0 0.5 fusion.29
  71.5 0.4 fusion.5
  72.0 0.4 fusion.4
  72.9 3.0 %collective-permute-done.3.q_ref = bf16[320,256]{1,0:T(8,128)(2,1)} collective-permute-done((bf16[320,256]{1,0:T(8,128)(2,1)S(1)}, bf16[320,256]{1,0:T(8,128)(2,1)}, u32[]{:S(2)}, u32[]{:S(2)}) %collective-permute-start.3) | collective-permute-done | bytes 163872 | tf_op jit(solution)/shard_map/ppermute | solution.py:223
  75.8 80.4 %all-gather.2.cloned.1.call-done.kv_ref = bf16[10240,256]{1,0:T(8,128)(2,1)} async-done(((bf16[320,256]{1,0:T(8,128)(2,1)}), bf16[10240,256]{1,0:T(8,128)(2,1)}) %all-gather.2.cloned.1.call-update) | async-done | bytes 5242896 | tf_op jit(solution)/shard_map/all_gather | solution.py:261
  156.2 13.5 %shard_map.111 = bf16[320,256]{1,0:T(8,128)(2,1)} custom-call(bf16[320,256]{1,0:T(8,128)(2,1)} %collective-permute-done.3.q_ref, bf16[10240,256]{1,0:T(8,128)(2,1)} %all-gather.2.cloned.1.call-done.kv_ref), custom_call_target="tpu_custom_call" | custom-call | flops 3355443200 | bytes 5242880 | tf_op jit(solution)/shard_map/pallas_call | solution.py:128
  169.7 1.9 collective-permute-start.4
  171.7 0.8 fusion.30
  172.5 4.0 %collective-permute-done.4 = bf16[320,256]{1,0:T(8,128)(2,1)S(1)} collective-permute-done((bf16[320,256]{1,0:T(8,128)(2,1)}, bf16[320,256]{1,0:T(8,128)(2,1)S(1)}, u32[]{:S(2)}, u32[]{:S(2)}) %collective-permute-start.4) | collective-permute-done | bytes 163872 | tf_op jit(solution)/shard_map/ppermute | solution.py:223
  176.6 0.9 fusion
  177.5 2.0 collective-permute-start.5
  179.5 3.0 %collective-permute-done.5 = bf16[160,4096]{1,0:T(8,128)(2,1)S(1)} collective-permute-done((bf16[160,4096]{1,0:T(8,128)(2,1)S(1)}, bf16[160,4096]{1,0:T(8,128)(2,1)S(1)}, u32[]{:S(2)}, u32[]{:S(2)}) %collective-permute-start.5) | collective-permute-done | bytes 1310752 | tf_op jit(solution)/shard_map/ppermute | solution.py:229
  182.5 0.4 add_convert_fusion
  183.0 2.0 collective-permute-start.6
  184.9 4.6 %collective-permute-start.8 = (bf16[40,4096]{1,0:T(8,128)(2,1)S(1)}, bf16[40,4096]{1,0:T(8,128)(2,1)S(1)}, u32[]{:S(2)}, u32[]{:S(2)}) collective-permute-start(bf16[40,4096]{1,0:T(8,128)(2,1)S(1)} %get-tuple-element.14), channel_id=1, source_target_pairs={{0,6},{2,0},{4,2},{6,4},{1,7},{3,1},{5,3},{7,5},{8,14},{10,8},{12,... | collective-permute-start | bytes 983048 | tf_op jit(solution)/shard_map/ppermute | solution.py:234
  189.5 2.3 %collective-permute-start.7 = (bf16[40,4096]{1,0:T(8,128)(2,1)S(1)}, bf16[40,4096]{1,0:T(8,128)(2,1)S(1)}, u32[]{:S(2)}, u32[]{:S(2)}) collective-permute-start(bf16[40,4096]{1,0:T(8,128)(2,1)S(1)} %get-tuple-element.15), channel_id=1, source_target_pairs={{0,4},{2,6},{4,0},{6,2},{1,5},{3,7},{5,1},{7,3},{8,12},{10,14},{12... | collective-permute-start | bytes 983048 | tf_op jit(solution)/shard_map/ppermute | solution.py:234
  191.9 3.3 %collective-permute-done.6 = bf16[40,4096]{1,0:T(8,128)(2,1)S(1)} collective-permute-done((bf16[40,4096]{1,0:T(8,128)(2,1)S(1)}, bf16[40,4096]{1,0:T(8,128)(2,1)S(1)}, u32[]{:S(2)}, u32[]{:S(2)}) %collective-permute-start.6) | collective-permute-done | bytes 327712 | tf_op jit(solution)/shard_map/ppermute | solution.py:234
  195.2 7.8 %collective-permute-done.8 = bf16[40,4096]{1,0:T(8,128)(2,1)S(1)} collective-permute-done((bf16[40,4096]{1,0:T(8,128)(2,1)S(1)}, bf16[40,4096]{1,0:T(8,128)(2,1)S(1)}, u32[]{:S(2)}, u32[]{:S(2)}) %collective-permute-start.8) | collective-permute-done | bytes 327712 | tf_op jit(solution)/shard_map/ppermute | solution.py:234
  203.1 0.9 add_convert_fusion.1
  (55 shorter events, 1.9 us)
Async XLA Ops:
  6.5 165.1 %copy-start = (bf16[256,4096]{1,0:T(8,128)(2,1)S(1)}, bf16[256,4096]{1,0:T(8,128)(2,1)}, u32[]{:S(2)}) copy-start(bf16[256,4096]{1,0:T(8,128)(2,1)} %param.20) | copy-start | bytes 6291460
  6.6 20.8 %copy-start.2 = (bf16[320,128]{1,0:T(8,128)(2,1)S(1)}, bf16[320,128]{1,0:T(8,128)(2,1)}, u32[]{:S(2)}) copy-start(bf16[320,128]{1,0:T(8,128)(2,1)} %param.13) | copy-start | bytes 245764
  6.6 20.8 %copy-start.3 = (bf16[320,128]{1,0:T(8,128)(2,1)S(1)}, bf16[320,128]{1,0:T(8,128)(2,1)}, u32[]{:S(2)}) copy-start(bf16[320,128]{1,0:T(8,128)(2,1)} %param.12) | copy-start | bytes 245764
  6.6 149.6 %all-gather.2.cloned.1.call-start = ((), (), s32[]{:S(2)}) async-start(), calls=%async_computation | async-start | bytes 5406720 | tf_op jit(solution)/shard_map/all_gather | solution.py:261
  10.2 8.9 %collective-permute-start.2 = (bf16[320,256]{1,0:T(8,128)(2,1)}, bf16[320,256]{1,0:T(8,128)(2,1)S(1)}, u32[]{:S(2)}, u32[]{:S(2)}) collective-permute-start(bf16[320,256]{1,0:T(8,128)(2,1)} %shard_map.109), channel_id=1, source_target_pairs={{0,0},{1,8},{2,2},{3,10},{4,4},{5,12},{6,6},{7,14},{8,1},{9,9},{10... | collective-permute-start | bytes 491528 | tf_op jit(solution)/shard_map/ppermute | solution.py:223
  19.1 0.7 copy-start.5
  20.7 6.0 %collective-permute-start.1 = (bf16[2,128,128]{2,1,0:T(8,128)(2,1)S(1)}, bf16[2,128,128]{2,1,0:T(8,128)(2,1)S(1)}, u32[]{:S(2)}, u32[]{:S(2)}) collective-permute-start(bf16[2,128,128]{2,1,0:T(8,128)(2,1)S(1)} %get-tuple-element.28), channel_id=1, source_target_pairs={{8,0},{16,8},{24,16},{32,24},{40,32},{48,40},{56,48},{64,56},{72,6... | collective-permute-start | bytes 196616 | tf_op jit(solution)/shard_map/ppermute | solution.py:161
  22.0 5.4 %collective-permute-start = (bf16[2,128,128]{2,1,0:T(8,128)(2,1)S(1)}, bf16[2,128,128]{2,1,0:T(8,128)(2,1)S(1)}, u32[]{:S(2)}, u32[]{:S(2)}) collective-permute-start(bf16[2,128,128]{2,1,0:T(8,128)(2,1)S(1)} %get-tuple-element.29), channel_id=1, source_target_pairs={{0,8},{8,16},{16,24},{24,32},{32,40},{40,48},{48,56},{56,64},{64,7... | collective-permute-start | bytes 196616 | tf_op jit(solution)/shard_map/ppermute | solution.py:159
  26.5 1.9 copy-start.4
  27.6 0.8 copy-start.6
  28.4 43.0 %copy-start.8 = (f32[2]{0:T(128)S(1)}, f32[2]{0:T(128)}, u32[]{:S(2)}) copy-start(f32[2]{0:T(128)} %param.17) | copy-start | bytes 28
  30.7 41.3 %copy-start.7 = (bf16[5,320,1,128]{3,1,0,2:T(8,128)(2,1)S(1)}, bf16[5,320,1,128]{3,1,0,2:T(8,128)(2,1)}, u32[]{:S(2)}) copy-start(bf16[5,320,1,128]{3,1,0,2:T(8,128)(2,1)} %copy-done.6) | copy-start | bytes 1228804
  31.9 43.9 %collective-permute-start.3 = (bf16[320,256]{1,0:T(8,128)(2,1)S(1)}, bf16[320,256]{1,0:T(8,128)(2,1)}, u32[]{:S(2)}, u32[]{:S(2)}) collective-permute-start(bf16[320,256]{1,0:T(8,128)(2,1)S(1)} %bitcast.72), channel_id=1, source_target_pairs={{0,0},{1,8},{2,2},{3,10},{4,4},{5,12},{6,6},{7,14},{8,1},{9,9},{10... | collective-permute-start | bytes 491528 | tf_op jit(solution)/shard_map/ppermute | solution.py:223
  169.7 6.9 %collective-permute-start.4 = (bf16[320,256]{1,0:T(8,128)(2,1)}, bf16[320,256]{1,0:T(8,128)(2,1)S(1)}, u32[]{:S(2)}, u32[]{:S(2)}) collective-permute-start(bf16[320,256]{1,0:T(8,128)(2,1)} %shard_map.111), channel_id=1, source_target_pairs={{0,0},{1,8},{2,2},{3,10},{4,4},{5,12},{6,6},{7,14},{8,1},{9,9},{10... | collective-permute-start | bytes 491528 | tf_op jit(solution)/shard_map/ppermute | solution.py:223
  171.7 4.9 %copy-start.1 = (bf16[256,4096]{1,0:T(8,128)(2,1)S(1)}, bf16[256,4096]{1,0:T(8,128)(2,1)}, u32[]{:S(2)}) copy-start(bf16[256,4096]{1,0:T(8,128)(2,1)} %param.21) | copy-start | bytes 6291460
  177.5 5.0 %collective-permute-start.5 = (bf16[160,4096]{1,0:T(8,128)(2,1)S(1)}, bf16[160,4096]{1,0:T(8,128)(2,1)S(1)}, u32[]{:S(2)}, u32[]{:S(2)}) collective-permute-start(bf16[160,4096]{1,0:T(8,128)(2,1)S(1)} %slice.141), channel_id=1, source_target_pairs={{0,1},{1,0},{2,3},{3,2},{4,5},{5,4},{6,7},{7,6},{8,9},{9,8},{10,11... | collective-permute-start | bytes 3932168 | tf_op jit(solution)/shard_map/ppermute | solution.py:229
  183.0 12.3 %collective-permute-start.6 = (bf16[40,4096]{1,0:T(8,128)(2,1)S(1)}, bf16[40,4096]{1,0:T(8,128)(2,1)S(1)}, u32[]{:S(2)}, u32[]{:S(2)}) collective-permute-start(bf16[40,4096]{1,0:T(8,128)(2,1)S(1)} %get-tuple-element.13), channel_id=1, source_target_pairs={{0,2},{2,4},{4,6},{6,0},{1,3},{3,5},{5,7},{7,1},{8,10},{10,12},{12... | collective-permute-start | bytes 983048 | tf_op jit(solution)/shard_map/ppermute | solution.py:234
  184.9 18.1 %collective-permute-start.8 = (bf16[40,4096]{1,0:T(8,128)(2,1)S(1)}, bf16[40,4096]{1,0:T(8,128)(2,1)S(1)}, u32[]{:S(2)}, u32[]{:S(2)}) collective-permute-start(bf16[40,4096]{1,0:T(8,128)(2,1)S(1)} %get-tuple-element.14), channel_id=1, source_target_pairs={{0,6},{2,0},{4,2},{6,4},{1,7},{3,1},{5,3},{7,5},{8,14},{10,8},{12,... | collective-permute-start | bytes 983048 | tf_op jit(solution)/shard_map/ppermute | solution.py:234
  189.5 13.5 %collective-permute-start.7 = (bf16[40,4096]{1,0:T(8,128)(2,1)S(1)}, bf16[40,4096]{1,0:T(8,128)(2,1)S(1)}, u32[]{:S(2)}, u32[]{:S(2)}) collective-permute-start(bf16[40,4096]{1,0:T(8,128)(2,1)S(1)} %get-tuple-element.15), channel_id=1, source_target_pairs={{0,4},{2,6},{4,0},{6,2},{1,5},{3,7},{5,1},{7,3},{8,12},{10,14},{12... | collective-permute-start | bytes 983048 | tf_op jit(solution)/shard_map/ppermute | solution.py:234
Sparse Core Ops, SparseCore 0:
  20.0 136.1 all-gather.1

commit v2 on v1

--- a/solution.py
+++ b/solution.py
@@ -18,6 +18,7 @@
 EPSILON = 1e-06
 CORES = 2
 PLANES = 2
+TAIL = 32
 
 
 def turn_tables(offset, local_rows):
@@ -64,16 +65,13 @@
     )(*args)
 
 
-def attend_kernel(q_ref, kv_ref, o_ref, rows_ref, top_ref, sum_ref, acc_ref, *, chunks):
+def attend_kernel(q_ref, kv_ref, o_ref, top_ref, sum_ref, acc_ref, *, chunks):
     step = pl.program_id(0)
-    heads = q_ref.shape[1] // HEAD
-    count = q_ref.shape[0]
+    rows = q_ref.shape[0]
     factor = math.log2(math.e) * HEAD ** (-0.5)
 
     @pl.when(step == 0)
     def _():
-        for h in range(heads):
-            rows_ref[h * count : (h + 1) * count, :] = q_ref[:, h * HEAD : (h + 1) * HEAD]
         top_ref[...] = jnp.full_like(top_ref, NEGATIVE)
         sum_ref[...] = jnp.zeros_like(sum_ref)
         acc_ref[...] = jnp.zeros_like(acc_ref)
@@ -84,7 +82,7 @@
     def score(lo, hi):
         return lax.dot_general(
             keys,
-            rows_ref[lo:hi, :],
+            q_ref[lo:hi, :],
             (((1,), (1,)), ((), ())),
             preferred_element_type=jnp.float32,
         )
@@ -113,29 +111,33 @@
 
     @pl.when(step == pl.num_programs(0) - 1)
     def _():
-        out = (acc_ref[...] / sum_ref[...]).T.astype(jnp.bfloat16)
-        for h in range(heads):
-            o_ref[:, h * HEAD : (h + 1) * HEAD] = out[h * count : (h + 1) * count, :]
+        weight = top_ref[...] * factor + jnp.log2(sum_ref[...])
+        high = weight.astype(jnp.bfloat16)
+        left = weight - high.astype(jnp.float32)
+        middle = left.astype(jnp.bfloat16)
+        low = (left - middle.astype(jnp.float32)).astype(jnp.bfloat16)
+        tail = [jnp.broadcast_to(t.astype(jnp.float32), (8, rows)) for t in (high, middle, low)]
+        tail.append(jnp.zeros((8, rows), jnp.float32))
+        o_ref[:HEAD, :] = (acc_ref[...] / sum_ref[...]).astype(jnp.bfloat16)
+        o_ref[HEAD:, :] = jnp.concatenate(tail, axis=0).astype(jnp.bfloat16)
 
 
 def attend(queries, kv, block=1024, chunk=256):
-    count, width = queries.shape
+    rows = queries.shape[0]
     total = kv.shape[0]
     while total % block:
         block //= 2
-    rows = count * (width // HEAD)
     chunks = tuple((lo, min(lo + chunk, rows)) for lo in range(0, rows, chunk))
     return pl.pallas_call(
         functools.partial(attend_kernel, chunks=chunks),
         grid=(total // block,),
         in_specs=[
-            pl.BlockSpec((count, width), lambda i: (0, 0)),
+            pl.BlockSpec((rows, HEAD), lambda i: (0, 0)),
             pl.BlockSpec((block, 2 * HEAD), lambda i: (i, 0)),
         ],
-        out_specs=pl.BlockSpec((count, width), lambda i: (0, 0)),
-        out_shape=jax.ShapeDtypeStruct((count, width), jnp.bfloat16),
+        out_specs=pl.BlockSpec((HEAD + TAIL, rows), lambda i: (0, 0)),
+        out_shape=jax.ShapeDtypeStruct((HEAD + TAIL, rows), jnp.bfloat16),
         scratch_shapes=[
-            pltpu.VMEM((rows, HEAD), jnp.bfloat16),
             pltpu.VMEM((1, rows), jnp.float32),
             pltpu.VMEM((1, rows), jnp.float32),
             pltpu.VMEM((HEAD, rows), jnp.float32),
@@ -147,6 +149,39 @@
             transcendentals=rows * total,
         ),
     )(queries, kv)
+
+
+def merge_kernel(*refs):
+    o_ref = refs[-1]
+    heads = o_ref.shape[1] // HEAD
+    count = o_ref.shape[0]
+    parts = refs[:-1]
+    weights = [
+        r[HEAD : HEAD + 8, :].astype(jnp.float32)[:1]
+        + r[HEAD + 8 : HEAD + 16, :].astype(jnp.float32)[:1]
+        + r[HEAD + 16 : HEAD + 24, :].astype(jnp.float32)[:1]
+        for r in parts
+    ]
+    top = functools.reduce(jnp.maximum, weights)
+    shares = [jnp.exp2(w - top) for w in weights]
+    total = functools.reduce(jnp.add, shares)
+    out = functools.reduce(
+        jnp.add, [r[:HEAD, :].astype(jnp.float32) * s for r, s in zip(parts, shares)]
+    )
+    out = (out / total).T.astype(jnp.bfloat16)
+    for h in range(heads):
+        o_ref[:, h * HEAD : (h + 1) * HEAD] = out[h * count : (h + 1) * count, :]
+
+
+def merged_parts(parts, heads):
+    count = parts[0].shape[1]
+    return pl.pallas_call(
+        merge_kernel,
+        out_shape=jax.ShapeDtypeStruct((count // heads, heads * HEAD), jnp.bfloat16),
+        cost_estimate=pl.CostEstimate(
+            flops=8 * count * HEAD, bytes_accessed=count * HEAD * 10, transcendentals=count
+        ),
+    )(*parts)
 
 
 def extended(cells, axes, width):
@@ -211,18 +246,6 @@
     return jnp.swapaxes(tiles, 0, 1).reshape(rows.shape)
 
 
-def swapped(value):
-    across = lax.axis_size("x")
-    index = lambda plane, x, core: (plane * across + x) * CORES + core
-    pairs = [
-        (index(p, x, c), index(c, x, p))
-        for p in range(PLANES)
-        for x in range(across)
-        for c in range(CORES)
-    ]
-    return lax.ppermute(value, ("lo", "x", "core"), pairs)
-
-
 def sent_and_summed(partial):
     half = partial.shape[0] // CORES
     across = lax.axis_size("x")
@@ -257,13 +280,19 @@
     offset = plane * local_rows
     total_rows = local_rows * lax.axis_size("hi") * PLANES
     cos, sin = turn_tables(offset, local_rows)
-    kv = swapped(turn(grid_key, key_gain, cos, sin, grid_value))
-    kv_all = lax.all_gather(kv, ("hi", "core"), axis=0, tiled=True)
+    kv = turn(grid_key, key_gain, cos, sin, grid_value)
+    kv_all = lax.all_gather(kv, "hi", axis=0, tiled=True)
 
     kv, cos, sin, grid_query, window_query = lax.optimization_barrier(
         (kv, cos, sin, grid_query, window_query)
     )
-    queries = swapped(by_target(turn(grid_query, query_gain, cos, sin)))
+    heads = grid_query.shape[1] // HEAD
+    turned = by_target(turn(grid_query, query_gain, cos, sin))
+    queries = jnp.concatenate(
+        [turned[:, h * HEAD : (h + 1) * HEAD] for h in range(heads)], axis=0
+    )
+    across = [(i, PLANES - 1 - i) for i in range(PLANES)]
+    queries_there = lax.ppermute(queries, "lo", across)
 
     local_heads = sink_logit.shape[0]
     head_number = head_group * local_heads + 1 + jnp.arange(local_heads, dtype=jnp.int32)
@@ -272,7 +301,9 @@
     window_out = by_target(
         window_attend(window_query, padded[0], padded[1], slopes, sink_logit, offset, total_rows)
     )
-    grid_out = swapped(attend(queries, kv_all))
+    part_there = attend(queries_there, kv_all)
+    part_back = lax.ppermute(part_there, "lo", across)
+    grid_out = merged_parts((attend(queries, kv_all), part_back), heads)
     partial = jnp.dot(window_out, window_weights, preferred_element_type=jnp.float32) + jnp.dot(
         grid_out, grid_weights, preferred_element_type=jnp.float32
     )

time: 212 us -> 218 us (1.028)
  starting transfers between devices: 63 us -> 34 us
  waiting for transfers between devices: 105 us -> 130 us
  matrix products: 2.56 us -> 7.99 us
  Pallas kernels: 17.7 us -> 21.3 us
    ppermute x3 -> x2, starting transfers between devices: 46.8 us -> 7.86 us  [the longest x1 4.44 us: per_device(): queries_there = lax.ppermute(queries, 'lo', across)]
    all_gather x1, waiting for transfers between devices: 80.4 us -> 118 us  [per_device(): kv_all = lax.all_gather(kv, 'hi', axis=0, tiled=True)]
    ppermute x3 -> x2, waiting for transfers between devices: 10.2 us -> 0.01 us  [the longest x1 0.01 us: per_device(): queries_there = lax.ppermute(queries, 'lo', across)]
    ppermute x1, starting transfers between devices: 1.95 us -> 10.3 us  [sent_and_summed(): theirs = lax.ppermute(partial[half:], 'core', [(0, 1), (1, 0)])]
    dot_general x1, matrix products: 0.86 us -> 4.03 us  [per_device(): jnp.dot(grid_out, grid_weights, preferred_element_type=jnp.float32)]
    dot_general x1, matrix products: 0.85 us -> 3.12 us  [per_device(): jnp.dot(window_out, window_weights, preferred_element_type=jnp.float32)]
    pallas_call x1 -> x2, Pallas kernels: 13.5 us -> 15.2 us  [attend(): pl.pallas_call(functools.partial(attend_kernel, chunks=chunks), grid=(tot...]
  transfers between devices with their start and end apart: 10 -> 9, of which waited for: 8 -> 5; matrix products, arithmetic and copies ran while one was open for 3% -> 4% of each run, Pallas kernels for 1% -> 6%
where the time goes in v2:
time: 218 us; the launch traced here: 215 us
  waiting for transfers between devices  130 us (60%)
  starting transfers between devices  34 us (16%)
  Pallas kernels  21.3 us (10%)
  between operations  13.9 us (6%)
  matrix products  7.99 us (4%)
  other arithmetic  6.22 us (3%)
    all_gather x1, waiting for transfers between devices, per_device(): kv_all = lax.all_gather(kv, 'hi', axis=0, tiled=True)  118 us
    pallas_call x2, Pallas kernels, attend(): pl.pallas_call(functools.partial(attend_kernel, chunks=chunks), grid=(tot...  15.2 us
    ppermute x1, starting transfers between devices, sent_and_summed(): theirs = lax.ppermute(partial[half:], 'core', [(0, 1), (1, 0)])  10.3 us
    ppermute x3, waiting for transfers between devices, sent_and_summed(): lax.ppermute(tiles[d], 'x', [(i, (i + d) % across) for i in range(across)])  9.9 us
    ppermute x3, starting transfers between devices, sent_and_summed(): lax.ppermute(tiles[d], 'x', [(i, (i + d) % across) for i in range(across)])  8.51 us
    ppermute x1, starting transfers between devices, extended(): lax.ppermute(tail, axes, [(i, i + 1) for i in range(ends)])  5.9 us
    ppermute x1, starting transfers between devices, per_device(): queries_there = lax.ppermute(queries, 'lo', across)  4.44 us
  transfers between devices with their start and end apart: 9, of which 5 were waited for; matrix products, arithmetic and copies ran while one was open for 4% of the time, Pallas kernels for 6%

profile of v2, /device:TPU:33, one launch (start us, length us, event | category | flops | bytes accessed | tf_op | source)
XLA Modules:
  0.0 215.2 jit_solution(3828916697977612418)
XLA Ops:
  6.6 1.0 pad_maximum_fusion.3
  7.5 1.4 collective-permute-start.1
  9.0 5.9 %collective-permute-start = (bf16[2,128,128]{2,1,0:T(8,128)(2,1)S(1)}, bf16[2,128,128]{2,1,0:T(8,128)(2,1)S(1)}, u32[]{:S(2)}, u32[]{:S(2)}) collective-permute-start(bf16[2,128,128]{2,1,0:T(8,128)(2,1)S(1)} %get-tuple-element.31), channel_id=1, source_target_pairs={{0,8},{8,16},{16,24},{24,32},{32,40},{40,48},{48,56},{56,64},{64,7... | collective-permute-start | bytes 196616 | tf_op jit(solution)/shard_map/ppermute | solution.py:194
  15.1 1.4 sine_multiply_fusion
  16.5 2.1 shard_map.109
  18.6 2.2 %shard_map.110 = bf16[320,256]{1,0:T(8,128)(2,1)} custom-call(bf16[320,256]{1,0:T(8,128)(2,1)} %x_ref.2, f32[1,128]{1,0:T(1,128)} %bitcast.74, f32[320,128]{1,0:T(8,128)} %get-tuple-element.11.cos_ref, f32[320,128]{1,0:T(8,128)} %get-tuple-element.12.sin_ref), custom_call_target="tpu_custom_call" | custom-call | flops 1310720 | bytes 655360 | tf_op jit(solution)/shard_map/pallas_call | solution.py:59
  20.8 1.0 reverse_select_fusion
  22.0 4.4 %collective-permute-start.2 = (bf16[640,128]{1,0:T(8,128)(2,1)S(1)}, bf16[640,128]{1,0:T(8,128)(2,1)S(1)}, u32[]{:S(2)}, u32[]{:S(2)}) collective-permute-start(bf16[640,128]{1,0:T(8,128)(2,1)S(1)} %pad_maximum_fusion.2.q_ref), channel_id=1, source_target_pairs={{0,8},{8,0},{1,9},{9,1},{2,10},{10,2},{3,11},{11,3},{4,12},{12,4},... | collective-permute-start | bytes 491528 | tf_op jit(solution)/shard_map/ppermute | solution.py:295
  26.7 0.2 fusion.10
  26.9 0.1 fusion.7
  27.5 0.5 fusion.30
  28.1 0.4 fusion.5
  28.6 0.4 fusion.4
  28.9 0.2 copy.19
  29.4 117.9 %all-gather.2.cloned.1.call-done.kv_ref = bf16[5120,256]{1,0:T(8,128)(2,1)} async-done(((bf16[320,256]{1,0:T(8,128)(2,1)}), bf16[5120,256]{1,0:T(8,128)(2,1)}) %all-gather.2.cloned.1.call-update) | async-done | bytes 2621456 | tf_op jit(solution)/shard_map/all_gather | solution.py:284
  147.3 7.6 %shard_map.112 = bf16[160,640]{1,0:T(8,128)(2,1)} custom-call(bf16[640,128]{1,0:T(8,128)(2,1)} %copy-done.7, bf16[5120,256]{1,0:T(8,128)(2,1)} %all-gather.2.cloned.1.call-done.kv_ref), custom_call_target="tpu_custom_call" | custom-call | flops 1677721600 | bytes 2621440 | tf_op jit(solution)/shard_map/pallas_call | solution.py:131
  154.9 3.4 %collective-permute-start.3 = (bf16[160,640]{1,0:T(8,128)(2,1)}, bf16[160,640]{1,0:T(8,128)(2,1)S(1)}, u32[]{:S(2)}, u32[]{:S(2)}) collective-permute-start(bf16[160,640]{1,0:T(8,128)(2,1)} %shard_map.112), channel_id=1, source_target_pairs={{0,8},{8,0},{1,9},{9,1},{2,10},{10,2},{3,11},{11,3},{4,12},{12,4},... | collective-permute-start | bytes 614408 | tf_op jit(solution)/shard_map/ppermute | solution.py:305
  158.3 3.1 %fusion.31 = f32[320,4096]{1,0:T(8,128)} fusion(bf16[320,256]{1,0:T(8,128)(2,1)S(1)} %bitcast.56, bf16[256,4096]{1,0:T(8,128)(2,1)S(1)} %copy-done), kind=kOutput, calls=%fused_computation.80 | convolution fusion | flops 671088640 | bytes 7503872 | tf_op jit(solution)/shard_map/dot_general | solution.py:307
  161.4 7.6 %shard_map.111.refs_0_ = bf16[160,640]{1,0:T(8,128)(2,1)} custom-call(bf16[640,128]{1,0:T(8,128)(2,1)} %copy-done.5, bf16[5120,256]{1,0:T(8,128)(2,1)} %all-gather.2.cloned.1.call-done.kv_ref), custom_call_target="tpu_custom_call" | custom-call | flops 1677721600 | bytes 2621440 | tf_op jit(solution)/shard_map/pallas_call | solution.py:131
  169.0 0.7 copy-done.3
  169.7 1.8 shard_map.113
  171.6 4.0 %fusion = bf16[320,4096]{1,0:T(8,128)(2,1)S(1)} fusion(f32[320,4096]{1,0:T(8,128)} %fusion.31, bf16[320,256]{1,0:T(8,128)(2,1)} %shard_map.113, bf16[256,4096]{1,0:T(8,128)(2,1)} %param.21), kind=kOutput, calls=%fused_computation.1 | convolution fusion | flops 673710080 | bytes 10125312 | tf_op jit(solution)/shard_map/dot_general | solution.py:307
  175.7 10.3 %collective-permute-start.4 = (bf16[160,4096]{1,0:T(8,128)(2,1)S(1)}, bf16[160,4096]{1,0:T(8,128)(2,1)S(1)}, u32[]{:S(2)}, u32[]{:S(2)}) collective-permute-start(bf16[160,4096]{1,0:T(8,128)(2,1)S(1)} %slice.151), channel_id=1, source_target_pairs={{0,1},{1,0},{2,3},{3,2},{4,5},{5,4},{6,7},{7,6},{8,9},{9,8},{10,11... | collective-permute-start | bytes 3932168 | tf_op jit(solution)/shard_map/ppermute | solution.py:252
  186.0 2.6 %collective-permute-done.4 = bf16[160,4096]{1,0:T(8,128)(2,1)S(1)} collective-permute-done((bf16[160,4096]{1,0:T(8,128)(2,1)S(1)}, bf16[160,4096]{1,0:T(8,128)(2,1)S(1)}, u32[]{:S(2)}, u32[]{:S(2)}) %collective-permute-start.4) | collective-permute-done | bytes 1310752 | tf_op jit(solution)/shard_map/ppermute | solution.py:252
  188.6 0.4 add_convert_fusion
  189.1 2.0 collective-permute-start.5
  191.0 4.6 %collective-permute-start.7 = (bf16[40,4096]{1,0:T(8,128)(2,1)S(1)}, bf16[40,4096]{1,0:T(8,128)(2,1)S(1)}, u32[]{:S(2)}, u32[]{:S(2)}) collective-permute-start(bf16[40,4096]{1,0:T(8,128)(2,1)S(1)} %get-tuple-element.14), channel_id=1, source_target_pairs={{0,6},{2,0},{4,2},{6,4},{1,7},{3,1},{5,3},{7,5},{8,14},{10,8},{12,... | collective-permute-start | bytes 983048 | tf_op jit(solution)/shard_map/ppermute | solution.py:257
  195.6 2.0 collective-permute-start.6
  197.6 3.5 %collective-permute-done.5 = bf16[40,4096]{1,0:T(8,128)(2,1)S(1)} collective-permute-done((bf16[40,4096]{1,0:T(8,128)(2,1)S(1)}, bf16[40,4096]{1,0:T(8,128)(2,1)S(1)}, u32[]{:S(2)}, u32[]{:S(2)}) %collective-permute-start.5) | collective-permute-done | bytes 327712 | tf_op jit(solution)/shard_map/ppermute | solution.py:257
  201.1 1.6 collective-permute-done.7
  202.7 4.8 %collective-permute-done.6 = bf16[40,4096]{1,0:T(8,128)(2,1)S(1)} collective-permute-done((bf16[40,4096]{1,0:T(8,128)(2,1)S(1)}, bf16[40,4096]{1,0:T(8,128)(2,1)S(1)}, u32[]{:S(2)}, u32[]{:S(2)}) %collective-permute-start.6) | collective-permute-done | bytes 327712 | tf_op jit(solution)/shard_map/ppermute | solution.py:257
  207.5 0.9 add_convert_fusion.1
  (55 shorter events, 1.4 us)
Async XLA Ops:
  6.5 151.7 %copy-start = (bf16[256,4096]{1,0:T(8,128)(2,1)S(1)}, bf16[256,4096]{1,0:T(8,128)(2,1)}, u32[]{:S(2)}) copy-start(bf16[256,4096]{1,0:T(8,128)(2,1)} %param.20) | copy-start | bytes 6291460
  6.6 140.7 %all-gather.2.cloned.1.call-start = ((), (), s32[]{:S(2)}) async-start(), calls=%async_computation | async-start | bytes 2785280 | tf_op jit(solution)/shard_map/all_gather | solution.py:284
  7.5 19.0 %copy-start.4 = (bf16[320,256]{1,0:T(8,128)(2,1)S(1)}, bf16[320,256]{1,0:T(8,128)(2,1)}, u32[]{:S(2)}) copy-start(bf16[320,256]{1,0:T(8,128)(2,1)} %param.11) | copy-start | bytes 491524
  7.5 19.6 %collective-permute-start.1 = (bf16[2,128,128]{2,1,0:T(8,128)(2,1)S(1)}, bf16[2,128,128]{2,1,0:T(8,128)(2,1)S(1)}, u32[]{:S(2)}, u32[]{:S(2)}) collective-permute-start(bf16[2,128,128]{2,1,0:T(8,128)(2,1)S(1)} %get-tuple-element.30), channel_id=1, source_target_pairs={{8,0},{16,8},{24,16},{32,24},{40,32},{48,40},{56,48},{64,56},{72,6... | collective-permute-start | bytes 196616 | tf_op jit(solution)/shard_map/ppermute | solution.py:196
  9.0 18.1 %collective-permute-start = (bf16[2,128,128]{2,1,0:T(8,128)(2,1)S(1)}, bf16[2,128,128]{2,1,0:T(8,128)(2,1)S(1)}, u32[]{:S(2)}, u32[]{:S(2)}) collective-permute-start(bf16[2,128,128]{2,1,0:T(8,128)(2,1)S(1)} %get-tuple-element.31), channel_id=1, source_target_pairs={{0,8},{8,16},{16,24},{24,32},{32,40},{40,48},{48,56},{56,64},{64,7... | collective-permute-start | bytes 196616 | tf_op jit(solution)/shard_map/ppermute | solution.py:194
  16.5 10.6 %copy-start.1 = (bf16[320,128]{1,0:T(8,128)(2,1)S(1)}, bf16[320,128]{1,0:T(8,128)(2,1)}, u32[]{:S(2)}) copy-start(bf16[320,128]{1,0:T(8,128)(2,1)} %param.13) | copy-start | bytes 245764
  16.5 10.6 %copy-start.2 = (bf16[320,128]{1,0:T(8,128)(2,1)S(1)}, bf16[320,128]{1,0:T(8,128)(2,1)}, u32[]{:S(2)}) copy-start(bf16[320,128]{1,0:T(8,128)(2,1)} %param.12) | copy-start | bytes 245764
  22.0 5.5 %copy-start.5 = (bf16[640,128]{1,0:T(8,128)(2,1)}, bf16[640,128]{1,0:T(8,128)(2,1)S(1)}, u32[]{:S(2)}) copy-start(bf16[640,128]{1,0:T(8,128)(2,1)S(1)} %pad_maximum_fusion.2.q_ref) | copy-start | bytes 491524
  22.0 7.4 %collective-permute-start.2 = (bf16[640,128]{1,0:T(8,128)(2,1)S(1)}, bf16[640,128]{1,0:T(8,128)(2,1)S(1)}, u32[]{:S(2)}, u32[]{:S(2)}) collective-permute-start(bf16[640,128]{1,0:T(8,128)(2,1)S(1)} %pad_maximum_fusion.2.q_ref), channel_id=1, source_target_pairs={{0,8},{8,0},{1,9},{9,1},{2,10},{10,2},{3,11},{11,3},{4,12},{12,4},... | collective-permute-start | bytes 491528 | tf_op jit(solution)/shard_map/ppermute | solution.py:295
  27.3 0.7 copy-start.6
  29.4 117.9 %copy-start.7 = (bf16[640,128]{1,0:T(8,128)(2,1)}, bf16[640,128]{1,0:T(8,128)(2,1)S(1)}, u32[]{:S(2)}) copy-start(bf16[640,128]{1,0:T(8,128)(2,1)S(1)} %collective-permute-done.2.q_ref) | copy-start | bytes 491524
  154.9 14.2 %collective-permute-start.3 = (bf16[160,640]{1,0:T(8,128)(2,1)}, bf16[160,640]{1,0:T(8,128)(2,1)S(1)}, u32[]{:S(2)}, u32[]{:S(2)}) collective-permute-start(bf16[160,640]{1,0:T(8,128)(2,1)} %shard_map.112), channel_id=1, source_target_pairs={{0,8},{8,0},{1,9},{9,1},{2,10},{10,2},{3,11},{11,3},{4,12},{12,4},... | collective-permute-start | bytes 614408 | tf_op jit(solution)/shard_map/ppermute | solution.py:305
  169.0 0.7 copy-start.3
  175.7 12.9 %collective-permute-start.4 = (bf16[160,4096]{1,0:T(8,128)(2,1)S(1)}, bf16[160,4096]{1,0:T(8,128)(2,1)S(1)}, u32[]{:S(2)}, u32[]{:S(2)}) collective-permute-start(bf16[160,4096]{1,0:T(8,128)(2,1)S(1)} %slice.151), channel_id=1, source_target_pairs={{0,1},{1,0},{2,3},{3,2},{4,5},{5,4},{6,7},{7,6},{8,9},{9,8},{10,11... | collective-permute-start | bytes 3932168 | tf_op jit(solution)/shard_map/ppermute | solution.py:252
  189.1 12.0 %collective-permute-start.5 = (bf16[40,4096]{1,0:T(8,128)(2,1)S(1)}, bf16[40,4096]{1,0:T(8,128)(2,1)S(1)}, u32[]{:S(2)}, u32[]{:S(2)}) collective-permute-start(bf16[40,4096]{1,0:T(8,128)(2,1)S(1)} %get-tuple-element.13), channel_id=1, source_target_pairs={{0,2},{2,4},{4,6},{6,0},{1,3},{3,5},{5,7},{7,1},{8,10},{10,12},{12... | collective-permute-start | bytes 983048 | tf_op jit(solution)/shard_map/ppermute | solution.py:257
  191.0 11.7 %collective-permute-start.7 = (bf16[40,4096]{1,0:T(8,128)(2,1)S(1)}, bf16[40,4096]{1,0:T(8,128)(2,1)S(1)}, u32[]{:S(2)}, u32[]{:S(2)}) collective-permute-start(bf16[40,4096]{1,0:T(8,128)(2,1)S(1)} %get-tuple-element.14), channel_id=1, source_target_pairs={{0,6},{2,0},{4,2},{6,4},{1,7},{3,1},{5,3},{7,5},{8,14},{10,8},{12,... | collective-permute-start | bytes 983048 | tf_op jit(solution)/shard_map/ppermute | solution.py:257
  195.6 11.9 %collective-permute-start.6 = (bf16[40,4096]{1,0:T(8,128)(2,1)S(1)}, bf16[40,4096]{1,0:T(8,128)(2,1)S(1)}, u32[]{:S(2)}, u32[]{:S(2)}) collective-permute-start(bf16[40,4096]{1,0:T(8,128)(2,1)S(1)} %get-tuple-element.15), channel_id=1, source_target_pairs={{0,4},{2,6},{4,0},{6,2},{1,5},{3,7},{5,1},{7,3},{8,12},{10,14},{12... | collective-permute-start | bytes 983048 | tf_op jit(solution)/shard_map/ppermute | solution.py:257
Sparse Core Ops, SparseCore 0:
  18.8 128.4 all-gather.1
